TPU v7x, 512 devices: a whole 4x4x16 slice. The times are simulated.
512 devices in a mesh: sp: 32 (over z, core), tp: 16 (over y, x).
Axes of the slice: x: 4, y: 4, z: 16, core: 2. Of those that a mesh axis runs over, the one named last changes fastest.
Arguments:
- b_gate: bfloat16 [8192, 1024], P('sp', 'tp'), may hold values from -6 to 6
- c_gate: bfloat16 [8192, 1024], P('sp', 'tp'), may hold values from -6 to 6
- h_in: bfloat16 [8192, 1024], P('sp', 'tp'), may hold values from -6 to 6
- docs: int32 [8192], replicated, may hold values from 0 to 15, never falling along the last dimension, each value on 1 to 1024 neighbouring positions
- conv_taps: bfloat16 [3, 1024], replicated, may hold values from -3 to 3
- out_weight: bfloat16 [1024, 4096], P(None, 'tp'), may hold values from -0.1875 to 0.1875
- residual_in: bfloat16 [8192, 4096], P('sp', 'tp'), may hold values from -52 to 52
- norm_gain: bfloat16 [4096], replicated, may hold values from 0.099609375 to 1.8984375
- expert_pick: int32 [8192, 2], P('sp'), may hold values from 0 to 31, as said below
- route_weight: float32 [8192, 2], P('sp'), may hold values from 0.5 to 2
- w_gate: bfloat16 [32, 4096, 2048], P('sp', None, 'tp'), may hold values from -0.09375 to 0.09375
- w_up: bfloat16 [32, 4096, 2048], P('sp', None, 'tp'), may hold values from -0.09375 to 0.09375
- w_down: bfloat16 [32, 2048, 4096], P('sp', None, 'tp'), may hold values from -0.125 to 0.125
Outputs:
- stream_out: bfloat16 [8192, 4096], P('sp', 'tp')
Inputs may be any that keep to these rules, and one draw needn't show every extreme that they name: `expert_pick`: each row names 2 different experts of one group; group g holds experts g * 8 up to the next group's first.
All inputs are finite; a program needn't handle non-finite values.
Results may differ from a plain program's by a relative error of at most 0.012.
Values may be sent and summed in bfloat16 or wider, within the bound.
No kernel may reach another device: no remote copies, remote signals or barrier semaphores. Data moves between devices by JAX's collectives and lax.ppermute only.
A program may use at most 64 MiB of HBM per device.

v0:
```python
import jax
import jax.numpy as jnp
from jax import lax
from jax.sharding import Mesh
from jax.sharding import PartitionSpec as P

TOP_K = 2
TP = ("tp_0", "tp_1")
NORM_EPS = 1e-06


def passed_along(value, axis, steps):
    count = lax.axis_size(axis)
    first, last = (max(0, -steps), min(count, count - steps))
    return lax.ppermute(value, axis, [(source, source + steps) for source in range(first, last)])


def laid_out(tiles, dim):
    shape = list(tiles.shape[1:])
    shape[dim] *= tiles.shape[0]
    return jnp.moveaxis(tiles, 0, dim).reshape(shape)


def from_everyone(shard, axis):
    devices = lax.axis_size(axis)
    return lax.all_to_all(
        jnp.broadcast_to(shard[None], (devices, *shard.shape)), axis, 0, 0, tiled=True
    )


def collect(shard, axis, dim):
    return laid_out(from_everyone(shard, axis), dim)


def by_axis(shard, axes):
    for axis in axes:
        shard = lax.psum(shard, axis)
    return shard


def local(
    b_gate,
    c_gate,
    h_in,
    docs,
    conv_taps,
    out_weight,
    residual_in,
    norm_gain,
    expert_pick,
    route_weight,
    w_gate,
    w_up,
    w_down,
):
    tok_rows, local_chans = h_in.shape
    width = residual_in.shape[1]
    full_dim = w_gate.shape[1]
    n_sp = lax.axis_size("sp")
    sp_index = lax.axis_index("sp")
    tp_index = lax.axis_index(TP)
    first_pos = sp_index * tok_rows
    product = (c_gate.astype(jnp.float32) * h_in.astype(jnp.float32)).astype(jnp.bfloat16)
    edge = passed_along(product[tok_rows - 2 :], "sp", 1)
    extended = jnp.concatenate([edge, product], axis=0).astype(jnp.float32)
    own_docs = lax.dynamic_slice_in_dim(docs, first_pos, tok_rows)
    padded_docs = jnp.concatenate([jnp.full((2,), -1, jnp.int32), docs], axis=0)
    near_docs = lax.dynamic_slice_in_dim(padded_docs, first_pos, tok_rows + 2)
    tap_weights = lax.dynamic_slice_in_dim(
        conv_taps, tp_index * local_chans, local_chans, 1
    ).astype(jnp.float32)
    conv_sum = tap_weights[0][None, :] * extended[2:]
    for step_back in (1, 2):
        same_doc = (near_docs[2 - step_back : 2 - step_back + tok_rows] == own_docs).astype(
            jnp.float32
        )[:, None]
        conv_sum = (
            conv_sum
            + tap_weights[step_back][None, :]
            * extended[2 - step_back : 2 - step_back + tok_rows]
            * same_doc
        )
    conv_out = (b_gate.astype(jnp.float32) * conv_sum).astype(jnp.bfloat16)
    projected = jnp.dot(collect(conv_out, TP, 1), out_weight, preferred_element_type=jnp.float32)
    stream = (residual_in.astype(jnp.float32) + projected).astype(jnp.bfloat16)
    stream_f = stream.astype(jnp.float32)
    capacity = 5 * tok_rows // (2 * n_sp)
    assign_flat = expert_pick.reshape(-1)
    onehot = (assign_flat[:, None] == jnp.arange(n_sp, dtype=jnp.int32)[None, :]).astype(jnp.int32)
    slot_pos = jnp.sum((jnp.cumsum(onehot, axis=0) - onehot) * onehot, axis=1)
    kept_mask = slot_pos < capacity
    target = jnp.where(
        kept_mask, assign_flat * capacity + jnp.minimum(slot_pos, capacity - 1), n_sp * capacity
    )
    table = (
        jnp.full((n_sp * capacity + 1,), -1, jnp.int32)
        .at[target]
        .set(jnp.arange(assign_flat.shape[0], dtype=jnp.int32))[:-1]
    )
    filled = table >= 0
    source_rows = jnp.maximum(table, 0) // TOP_K
    gate_local = w_gate[0]
    up_local = w_up[0]
    slot_rows = n_sp * capacity
    squares = by_axis(jnp.sum(stream_f * stream_f, axis=1), TP)
    inverse = lax.rsqrt(squares / full_dim + NORM_EPS)[:, None]
    gain_cols = lax.dynamic_slice_in_dim(norm_gain, tp_index * width, width).astype(jnp.float32)
    normed = (stream_f * inverse * gain_cols[None, :]).astype(jnp.bfloat16)
    outgoing = jnp.where(filled[:, None], normed[source_rows], jnp.zeros((), normed.dtype)).reshape(
        n_sp, capacity, width
    )
    received = lax.all_to_all(outgoing, "sp", split_axis=0, concat_axis=0, tiled=True)
    shard_piece = lax.all_gather(received, TP, axis=2, tiled=True)
    flat_piece = shard_piece.reshape(slot_rows, shard_piece.shape[2])
    gate_pre = jnp.dot(flat_piece, gate_local, preferred_element_type=jnp.float32)
    up_pre = jnp.dot(flat_piece, up_local, preferred_element_type=jnp.float32)
    hidden = (jax.nn.silu(gate_pre) * up_pre).astype(jnp.bfloat16)
    down_local = w_down[0]
    result = jnp.dot(collect(hidden, TP, 1), down_local, preferred_element_type=jnp.float32).astype(
        jnp.bfloat16
    )
    returned = lax.all_to_all(
        result.reshape(n_sp, capacity, width), "sp", split_axis=0, concat_axis=0, tiled=True
    ).reshape(n_sp * capacity, width)
    picked = jnp.where(
        kept_mask[:, None],
        returned[jnp.minimum(target, n_sp * capacity - 1)].astype(jnp.float32),
        0.0,
    )
    weighted = picked * route_weight.reshape(-1)[:, None]
    feed_out = jnp.sum(weighted.reshape(tok_rows, TOP_K, width), axis=1)
    return (stream_f + feed_out).astype(jnp.bfloat16)


def solution(mesh):
    finer = Mesh(mesh.devices.reshape(mesh.shape["sp"], 4, 4), ("sp", "tp_0", "tp_1"))
    placed = (
        P("sp", TP),
        P("sp", TP),
        P("sp", TP),
        P(),
        P(),
        P(None, TP),
        P("sp", TP),
        P(),
        P("sp", None),
        P("sp", None),
        P("sp", None, TP),
        P("sp", None, TP),
        P("sp", None, TP),
    )
    return jax.shard_map(local, mesh=finer, in_specs=placed, out_specs=P("sp", TP), check_vma=False)
```

profile of v0, /device:TPU:1, one launch (start us, length us, event | category | flops | bytes accessed | tf_op | source)
XLA Modules:
  0.0 282.6 jit_solution(15302591660513541208)
XLA Ops:
  6.5 0.9 multiply_convert_fusion.1
  7.5 4.9 %collective-permute-start = (bf16[2,64]{0,1:T(8,128)(2,1)S(1)}, bf16[2,64]{0,1:T(8,128)(2,1)S(1)}, u32[]{:S(2)}, u32[]{:S(2)}) collective-permute-start(bf16[2,64]{0,1:T(8,128)(2,1)S(1)} %slice.52), channel_id=1, source_target_pairs={{0,16},{16,32},{32,48},{48,64},{64,80},{80,96},{96,112},{112,128},... | collective-permute-start | bytes 776 | tf_op jit(solution)/shard_map/ppermute | solution.py:15
  12.4 0.8 copy.29
  13.5 1.2 reduce-window.6
  15.1 0.7 broadcast_multiply_fusion
  15.8 0.7 dynamic-slice_convert_fusion
  16.8 0.8 pad_dynamic-slice_fusion
  17.6 0.8 compare_convert_fusion.1
  18.4 2.4 scatter_custom_fusion
  21.0 0.9 fusion.13
  21.9 0.8 broadcast_in_dim.32
  22.7 6.8 %all-to-all-start = ((bf16[16,256,64]{1,2,0:T(8,128)(2,1)}), bf16[16,256,64]{1,2,0:T(8,128)(2,1)S(1)}, u32[]{:S(2)}, u32[]{:S(2)}) async-start(bf16[16,256,64]{1,2,0:T(8,128)(2,1)} %broadcast_in_dim.32), calls=%async_computation | async-start | bytes 1048576 | tf_op jit(solution)/shard_map/all_to_all | solution.py:26
  29.5 1.0 copy.28
  30.7 0.8 dynamic-slice_convert_fusion.1
  31.4 9.4 %all-to-all-done = bf16[16,256,64]{1,2,0:T(8,128)(2,1)S(1)} async-done(((bf16[16,256,64]{1,2,0:T(8,128)(2,1)}), bf16[16,256,64]{1,2,0:T(8,128)(2,1)S(1)}, u32[]{:S(2)}, u32[]{:S(2)}) %all-to-all-start) | async-done | bytes 524320 | tf_op jit(solution)/shard_map/all_to_all | solution.py:26
  40.8 1.4 multiply_reduce_fusion.1
  42.2 6.9 %psum.14 = f32[256]{0:T(256)S(1)} all-reduce(f32[256]{0:T(256)S(1)} %get-tuple-element.12), channel_id=1, replica_groups=mesh['sp'=32,'tp_0'=4,'tp_1'=4] {'tp_0'}, use_global_device_ids=true, to_apply=%region_5.6 | all-reduce | flops 256 | bytes 2048 | tf_op jit(solution)/shard_map/psum | solution.py:37
  49.1 6.3 %psum.15 = f32[256]{0:T(256)S(1)} all-reduce(f32[256]{0:T(256)S(1)} %psum.14), channel_id=1, replica_groups=mesh['sp'=32,'tp_0'=4,'tp_1'=4] {'tp_1'}, use_global_device_ids=true, to_apply=%region_6.7 | all-reduce | flops 256 | bytes 2048 | tf_op jit(solution)/shard_map/psum | solution.py:37
  55.6 2.8 gather_fusion
  58.7 47.2 %all_to_all.20 = bf16[32,20,256]{2,1,0:T(8,128)(2,1)} all-to-all(bf16[32,20,256]{2,1,0:T(8,128)(2,1)S(1)} %broadcast_select_fusion), channel_id=1, replica_groups=mesh['sp'=32,'tp_0'=4,'tp_1'=4] {'sp'}, dimensions={0} | all-to-all | bytes 655360 | tf_op jit(solution)/shard_map/all_to_all | solution.py:112
  105.9 68.7 %all-gather.2.cloned.1.call-done = bf16[32,20,4096]{2,1,0:T(8,128)(2,1)} async-done(((bf16[32,20,256]{2,1,0:T(8,128)(2,1)}), bf16[32,20,4096]{2,1,0:T(8,128)(2,1)}) %all-gather.2.cloned.1.call-update) | async-done | bytes 5242896 | tf_op jit(solution)/shard_map/all_gather | solution.py:113
  174.6 7.8 %reshape.133 = bf16[640,4096]{1,0:T(8,128)(2,1)} reshape(bf16[32,20,4096]{2,1,0:T(8,128)(2,1)} %all-gather.2.cloned.1.call-done) | data formatting | bytes 10485760 | tf_op jit(solution)/shard_map/reshape | solution.py:114
  182.5 4.1 %fusion.5 = f32[640,128]{1,0:T(8,128)S(1)} fusion(bf16[640,4096]{1,0:T(8,128)(2,1)} %reshape.133, bf16[1,4096,128]{2,1,0:T(8,128)(2,1)S(1)} %copy-done.3), kind=kOutput, calls=%fused_computation.11 | convolution fusion | flops 671088640 | bytes 6619136 | tf_op jit(solution)/shard_map/dot_general | solution.py:115
  186.8 1.5 fusion
  188.8 37.3 %all_to_all.21 = bf16[16,640,128]{1,2,0:T(8,128)(2,1)S(1)} all-to-all(bf16[16,640,128]{1,2,0:T(8,128)(2,1)S(1)} %broadcast_in_dim.62), channel_id=1, replica_groups=mesh['sp'=32,'tp_0'=4,'tp_1'=4] {'tp_0','tp_1'}, dimensions={0} | all-to-all | bytes 5242880 | tf_op jit(solution)/shard_map/all_to_all | solution.py:26
  226.2 0.9 convolution_convert_fusion
  227.1 0.8 reshape.135
  227.9 15.4 %all-to-all-start.3 = ((bf16[32,20,256]{2,1,0:T(8,128)(2,1)}), bf16[32,20,256]{2,1,0:T(8,128)(2,1)S(1)}, u32[]{:S(2)}, u32[]{:S(2)}) async-start(bf16[32,20,256]{2,1,0:T(8,128)(2,1)} %reshape.135), calls=%async_computation.3 | async-start | bytes 786432 | tf_op jit(solution)/shard_map/all_to_all | solution.py:122
  243.6 27.4 %all-to-all-done.3 = bf16[32,20,256]{2,1,0:T(8,128)(2,1)S(1)} async-done(((bf16[32,20,256]{2,1,0:T(8,128)(2,1)}), bf16[32,20,256]{2,1,0:T(8,128)(2,1)S(1)}, u32[]{:S(2)}, u32[]{:S(2)}) %all-to-all-start.3) | async-done | bytes 327712 | tf_op jit(solution)/shard_map/all_to_all | solution.py:122
  271.1 2.0 gather_fusion.1
  273.4 1.5 multiply_reduce_fusion
  275.0 0.8 copy.37
  (47 shorter events, 3.2 us)
Async XLA Ops:
  6.5 219.6 %copy-start = (bf16[1,2048,256]{2,1,0:T(8,128)(2,1)S(1)}, bf16[1,2048,256]{2,1,0:T(8,128)(2,1)}, u32[]{:S(2)}) copy-start(bf16[1,2048,256]{2,1,0:T(8,128)(2,1)} %param.25) | copy-start | bytes 3145732
  7.5 13.4 %collective-permute-start = (bf16[2,64]{0,1:T(8,128)(2,1)S(1)}, bf16[2,64]{0,1:T(8,128)(2,1)S(1)}, u32[]{:S(2)}, u32[]{:S(2)}) collective-permute-start(bf16[2,64]{0,1:T(8,128)(2,1)S(1)} %slice.52), channel_id=1, source_target_pairs={{0,16},{16,32},{32,48},{48,64},{64,80},{80,96},{96,112},{112,128},... | collective-permute-start | bytes 776 | tf_op jit(solution)/shard_map/ppermute | solution.py:15
  22.7 18.1 %all-to-all-start = ((bf16[16,256,64]{1,2,0:T(8,128)(2,1)}), bf16[16,256,64]{1,2,0:T(8,128)(2,1)S(1)}, u32[]{:S(2)}, u32[]{:S(2)}) async-start(bf16[16,256,64]{1,2,0:T(8,128)(2,1)} %broadcast_in_dim.32), calls=%async_computation | async-start | bytes 1048576 | tf_op jit(solution)/shard_map/all_to_all | solution.py:26
  29.5 145.2 %all-gather.2.cloned.1.call-start = ((), (), s32[]{:S(2)}) async-start(), calls=%async_computation.4 | async-start | bytes 6684672 | tf_op jit(solution)/shard_map/all_gather | solution.py:113
  105.9 76.5 %copy-start.3 = (bf16[1,4096,128]{2,1,0:T(8,128)(2,1)S(1)}, bf16[1,4096,128]{2,1,0:T(8,128)(2,1)}, u32[]{:S(2)}) copy-start(bf16[1,4096,128]{2,1,0:T(8,128)(2,1)} %param.23) | copy-start | bytes 3145732
  182.5 4.2 %copy-start.1 = (bf16[640,4096]{1,0:T(8,128)(2,1)S(1)}, bf16[640,4096]{1,0:T(8,128)(2,1)}, u32[]{:S(2)}) copy-start(bf16[640,4096]{1,0:T(8,128)(2,1)} %reshape.133) | copy-start | bytes 15728644
  182.5 4.3 %copy-start.4 = (bf16[1,4096,128]{2,1,0:T(8,128)(2,1)S(1)}, bf16[1,4096,128]{2,1,0:T(8,128)(2,1)}, u32[]{:S(2)}) copy-start(bf16[1,4096,128]{2,1,0:T(8,128)(2,1)} %param.24) | copy-start | bytes 3145732
  226.2 17.3 %copy-start.2 = (f32[256,2]{0,1:T(2,128)S(1)}, f32[256,2]{0,1:T(2,128)}, u32[]{:S(2)}) copy-start(f32[256,2]{0,1:T(2,128)} %param.22) | copy-start | bytes 6148
  227.9 43.2 %all-to-all-start.3 = ((bf16[32,20,256]{2,1,0:T(8,128)(2,1)}), bf16[32,20,256]{2,1,0:T(8,128)(2,1)S(1)}, u32[]{:S(2)}, u32[]{:S(2)}) async-start(bf16[32,20,256]{2,1,0:T(8,128)(2,1)} %reshape.135), calls=%async_computation.3 | async-start | bytes 786432 | tf_op jit(solution)/shard_map/all_to_all | solution.py:122
Sparse Core Ops, SparseCore 0:
  106.1 68.5 all-gather.1
where the time goes:
time: 284 us; the launch traced here: 283 us
  waiting for transfers between devices  106 us (37%)
  blocking collectives  97.8 us (34%)
  starting transfers between devices  27.1 us (10%)
  local copies, waits for them, and re-layouts  22.6 us (8%)
  between operations  13.7 us (5%)
  other arithmetic  7.98 us (3%)
  matrix products  7.96 us (3%)
    all_gather x1, waiting for transfers between devices, local(): shard_piece = lax.all_gather(received, TP, axis=2, tiled=True)  68.7 us
    all_to_all x1, blocking collectives, local(): lax.all_to_all(outgoing, 'sp', split_axis=0, concat_axis=0, tiled=True)  47.2 us
    all_to_all x1, blocking collectives, from_everyone(): lax.all_to_all(jnp.broadcast_to(shard[None], (devices, *shard.shape)), ax...  37.3 us
    all_to_all x1, waiting for transfers between devices, local(): lax.all_to_all(result.reshape(n_sp, capacity, width), 'sp', split_axis=0,...  27.4 us
    all_to_all x1, starting transfers between devices, local(): lax.all_to_all(result.reshape(n_sp, capacity, width), 'sp', split_axis=0,...  15.4 us
    psum x2, blocking collectives, by_axis(): shard = lax.psum(shard, axis)  13.2 us
    all_to_all x1, waiting for transfers between devices, from_everyone(): lax.all_to_all(jnp.broadcast_to(shard[None], (devices, *shard.shape)), ax...  9.4 us
    reshape x1, local copies, waits for them, and re-layouts, local(): flat_piece = shard_piece.reshape(slot_rows, shard_piece.shape[2])  7.84 us
  transfers between devices with their start and end apart: 4, of which 3 were waited for; matrix products, arithmetic and copies ran while one was open for 4% of the time, Pallas kernels for 0%

commit v1 on v0

--- a/solution.py
+++ b/solution.py
@@ -110,7 +110,9 @@
         n_sp, capacity, width
     )
     received = lax.all_to_all(outgoing, "sp", split_axis=0, concat_axis=0, tiled=True)
-    shard_piece = lax.all_gather(received, TP, axis=2, tiled=True)
+    shard_piece = jnp.concatenate(
+        lax.all_to_all(jnp.stack([received] * lax.axis_size(TP)), TP, 0, 0), axis=2
+    )
     flat_piece = shard_piece.reshape(slot_rows, shard_piece.shape[2])
     gate_pre = jnp.dot(flat_piece, gate_local, preferred_element_type=jnp.float32)
     up_pre = jnp.dot(flat_piece, up_local, preferred_element_type=jnp.float32)

time: 284 us -> 251 us (0.88)
  waiting for transfers between devices: 106 us -> 36.9 us
  blocking collectives: 97.8 us -> 160 us
  between operations: 13.7 us -> 0.34 us
  starting transfers between devices: 27.1 us -> 18.2 us
    all_gather x1 -> x0, waiting for transfers between devices: 68.7 us -> none  [local(): shard_piece = lax.all_gather(received, TP, axis=2, tiled=True)]
    all_to_all x0 -> x1, blocking collectives: none -> 63.8 us  [local(): lax.all_to_all(jnp.stack([received] * lax.axis_size(TP)), TP, 0, 0)]
    all_to_all x1, starting transfers between devices: 15.4 us -> 6.57 us  [local(): lax.all_to_all(result.reshape(n_sp, capacity, width), 'sp', split_axis=0,...]
    reshape x1, local copies, waits for them, and re-layouts: 7.84 us -> 2.97 us  [local(): jnp.concatenate(lax.all_to_all(jnp.stack([received] * lax.axis_size(TP)),...]
    unnamed x13 -> x12, local copies, waits for them, and re-layouts: 2.13 us -> 5.48 us
  transfers between devices with their start and end apart: 4 -> 3, of which waited for: 3 -> 2; matrix products, arithmetic and copies ran while one was open for 4% -> 4% of each run, Pallas kernels for 0% -> 0%
where the time goes in v1:
time: 251 us
  blocking collectives  160 us (64%)
  waiting for transfers between devices  36.9 us (15%)
  local copies, waits for them, and re-layouts  21.8 us (9%)
  starting transfers between devices  18.2 us (7%)
  other arithmetic  7.98 us (3%)
  matrix products  5.31 us (2%)
    all_to_all x1, blocking collectives, local(): lax.all_to_all(jnp.stack([received] * lax.axis_size(TP)), TP, 0, 0)  63.8 us
    all_to_all x1, blocking collectives, local(): lax.all_to_all(outgoing, 'sp', split_axis=0, concat_axis=0, tiled=True)  47.1 us
    all_to_all x1, blocking collectives, from_everyone(): lax.all_to_all(jnp.broadcast_to(shard[None], (devices, *shard.shape)), ax...  36 us
    all_to_all x1, waiting for transfers between devices, local(): lax.all_to_all(result.reshape(n_sp, capacity, width), 'sp', split_axis=0,...  27.4 us
    psum x2, blocking collectives, by_axis(): shard = lax.psum(shard, axis)  13.2 us
    all_to_all x1, waiting for transfers between devices, from_everyone(): lax.all_to_all(jnp.broadcast_to(shard[None], (devices, *shard.shape)), ax...  9.45 us
    all_to_all x1, starting transfers between devices, from_everyone(): lax.all_to_all(jnp.broadcast_to(shard[None], (devices, *shard.shape)), ax...  6.75 us
    all_to_all x1, starting transfers between devices, local(): lax.all_to_all(result.reshape(n_sp, capacity, width), 'sp', split_axis=0,...  6.57 us
  transfers between devices with their start and end apart: 3, of which 2 were waited for; matrix products, arithmetic and copies ran while one was open for 4% of the time, Pallas kernels for 0%

profile of v1, /device:TPU:1, one launch (start us, length us, event | category | flops | bytes accessed | tf_op | source)
XLA Modules:
  0.0 250.6 jit_solution(14769073404117762079)
XLA Ops:
  0.0 0.9 multiply_convert_fusion.1
  1.0 4.9 %collective-permute-start = (bf16[2,64]{0,1:T(8,128)(2,1)S(1)}, bf16[2,64]{0,1:T(8,128)(2,1)S(1)}, u32[]{:S(2)}, u32[]{:S(2)}) collective-permute-start(bf16[2,64]{0,1:T(8,128)(2,1)S(1)} %slice.52), channel_id=1, source_target_pairs={{0,16},{16,32},{32,48},{48,64},{64,80},{80,96},{96,112},{112,128},... | collective-permute-start | bytes 776 | tf_op jit(solution)/shard_map/ppermute | solution.py:15
  5.9 0.8 copy.40
  7.0 1.2 reduce-window.6
  9.3 0.7 dynamic-slice_convert_fusion
  10.3 0.8 pad_dynamic-slice_fusion
  11.1 0.8 compare_convert_fusion.1
  11.9 2.4 scatter_custom_fusion
  14.4 0.9 fusion.13
  15.3 0.8 broadcast_in_dim.32
  16.2 6.8 %all-to-all-start = ((bf16[16,256,64]{1,2,0:T(8,128)(2,1)}), bf16[16,256,64]{1,2,0:T(8,128)(2,1)S(1)}, u32[]{:S(2)}, u32[]{:S(2)}) async-start(bf16[16,256,64]{1,2,0:T(8,128)(2,1)} %broadcast_in_dim.32), calls=%async_computation | async-start | bytes 1048576 | tf_op jit(solution)/shard_map/all_to_all | solution.py:26
  22.9 1.0 copy.39
  24.1 0.8 dynamic-slice_convert_fusion.1
  24.8 9.4 %all-to-all-done = bf16[16,256,64]{1,2,0:T(8,128)(2,1)S(1)} async-done(((bf16[16,256,64]{1,2,0:T(8,128)(2,1)}), bf16[16,256,64]{1,2,0:T(8,128)(2,1)S(1)}, u32[]{:S(2)}, u32[]{:S(2)}) %all-to-all-start) | async-done | bytes 524320 | tf_op jit(solution)/shard_map/all_to_all | solution.py:26
  34.3 1.4 multiply_reduce_fusion.1
  35.7 6.9 %psum.14 = f32[256]{0:T(256)S(1)} all-reduce(f32[256]{0:T(256)S(1)} %get-tuple-element.12), channel_id=1, replica_groups=mesh['sp'=32,'tp_0'=4,'tp_1'=4] {'tp_0'}, use_global_device_ids=true, to_apply=%region_5.6 | all-reduce | flops 256 | bytes 2048 | tf_op jit(solution)/shard_map/psum | solution.py:37
  42.6 6.3 %psum.15 = f32[256]{0:T(256)S(1)} all-reduce(f32[256]{0:T(256)S(1)} %psum.14), channel_id=1, replica_groups=mesh['sp'=32,'tp_0'=4,'tp_1'=4] {'tp_1'}, use_global_device_ids=true, to_apply=%region_6.7 | all-reduce | flops 256 | bytes 2048 | tf_op jit(solution)/shard_map/psum | solution.py:37
  49.1 2.8 %gather_fusion = bf16[640,256]{1,0:T(8,128)(2,1)S(1)} fusion(bf16[256,256]{1,0:T(8,128)(2,1)S(1)} %copy.44, s32[1024]{0:T(1024)S(1)} %pad_clamp_fusion.1), kind=kCustom, calls=%fused_computation | custom fusion | bytes 657920 | tf_op jit(solution)/shard_map/gather | solution.py:109
  52.1 47.1 %all_to_all.25 = bf16[32,20,256]{2,1,0:T(8,128)(2,1)S(1)} all-to-all(bf16[32,20,256]{2,1,0:T(8,128)(2,1)S(1)} %broadcast_select_fusion), channel_id=1, replica_groups=mesh['sp'=32,'tp_0'=4,'tp_1'=4] {'sp'}, dimensions={0} | all-to-all | bytes 655360 | tf_op jit(solution)/shard_map/all_to_all | solution.py:112
  100.0 63.8 %all_to_all.26 = bf16[16,32,20,256]{3,1,2,0:T(8,128)(2,1)S(1)} all-to-all(bf16[16,32,20,256]{3,1,2,0:T(8,128)(2,1)S(1)} %stack.2), channel_id=1, replica_groups=mesh['sp'=32,'tp_0'=4,'tp_1'=4] {'tp_0','tp_1'}, dimensions={0} | all-to-all | bytes 10485760 | tf_op jit(solution)/shard_map/all_to_all | solution.py:114
  163.8 3.0 %copy.46 = bf16[32,20,16,256]{3,2,1,0:T(8,128)(2,1)S(1)} copy(bf16[32,20,16,256]{3,0,1,2:T(8,128)(2,1)S(1)} %bitcast.52) | data formatting | bytes 10485760 | tf_op jit(solution)/shard_map/reshape | solution.py:113
  166.8 3.5 %copy.52 = bf16[80,8,16,256]{3,1,2,0:T(8,128)(2,1)S(1)} copy(bf16[80,8,16,256]{3,2,1,0:T(8,128)(2,1)S(1)} %bitcast.53) | data formatting | bytes 10485760
  170.3 1.5 fusion.5
  171.9 1.5 fusion
  173.8 36.0 %all_to_all.27 = bf16[16,640,128]{1,2,0:T(8,128)(2,1)S(1)} all-to-all(bf16[16,640,128]{1,2,0:T(8,128)(2,1)S(1)} %broadcast_in_dim.62), channel_id=1, replica_groups=mesh['sp'=32,'tp_0'=4,'tp_1'=4] {'tp_0','tp_1'}, dimensions={0} | all-to-all | bytes 5242880 | tf_op jit(solution)/shard_map/all_to_all | solution.py:26
  209.8 0.9 convolution_convert_fusion
  210.7 0.8 reshape.137
  211.5 6.6 %all-to-all-start.4 = ((bf16[32,20,256]{2,1,0:T(8,128)(2,1)}), bf16[32,20,256]{2,1,0:T(8,128)(2,1)S(1)}, u32[]{:S(2)}, u32[]{:S(2)}) async-start(bf16[32,20,256]{2,1,0:T(8,128)(2,1)} %reshape.137), calls=%async_computation.4 | async-start | bytes 786432 | tf_op jit(solution)/shard_map/all_to_all | solution.py:124
  218.4 27.4 %all-to-all-done.4 = bf16[32,20,256]{2,1,0:T(8,128)(2,1)S(1)} async-done(((bf16[32,20,256]{2,1,0:T(8,128)(2,1)}), bf16[32,20,256]{2,1,0:T(8,128)(2,1)S(1)}, u32[]{:S(2)}, u32[]{:S(2)}) %all-to-all-start.4) | async-done | bytes 327712 | tf_op jit(solution)/shard_map/all_to_all | solution.py:124
  245.9 2.0 gather_fusion.1
  248.2 1.5 multiply_reduce_fusion
  249.8 0.8 copy.50
  (46 shorter events, 4.4 us)
Async XLA Ops:
  0.0 209.8 %copy-start = (bf16[1,2048,256]{2,1,0:T(8,128)(2,1)S(1)}, bf16[1,2048,256]{2,1,0:T(8,128)(2,1)}, u32[]{:S(2)}) copy-start(bf16[1,2048,256]{2,1,0:T(8,128)(2,1)} %param.25) | copy-start | bytes 3145732
  1.0 13.4 %collective-permute-start = (bf16[2,64]{0,1:T(8,128)(2,1)S(1)}, bf16[2,64]{0,1:T(8,128)(2,1)S(1)}, u32[]{:S(2)}, u32[]{:S(2)}) collective-permute-start(bf16[2,64]{0,1:T(8,128)(2,1)S(1)} %slice.52), channel_id=1, source_target_pairs={{0,16},{16,32},{32,48},{48,64},{64,80},{80,96},{96,112},{112,128},... | collective-permute-start | bytes 776 | tf_op jit(solution)/shard_map/ppermute | solution.py:15
  16.2 18.1 %all-to-all-start = ((bf16[16,256,64]{1,2,0:T(8,128)(2,1)}), bf16[16,256,64]{1,2,0:T(8,128)(2,1)S(1)}, u32[]{:S(2)}, u32[]{:S(2)}) async-start(bf16[16,256,64]{1,2,0:T(8,128)(2,1)} %broadcast_in_dim.32), calls=%async_computation | async-start | bytes 1048576 | tf_op jit(solution)/shard_map/all_to_all | solution.py:26
  166.8 3.5 %copy-start.2 = (bf16[1,4096,128]{2,1,0:T(8,128)(2,1)S(1)}, bf16[1,4096,128]{2,1,0:T(8,128)(2,1)}, u32[]{:S(2)}) copy-start(bf16[1,4096,128]{2,1,0:T(8,128)(2,1)} %param.23) | copy-start | bytes 3145732
  170.3 1.5 copy-start.3
  209.8 8.5 %copy-start.1 = (f32[256,2]{0,1:T(2,128)S(1)}, f32[256,2]{0,1:T(2,128)}, u32[]{:S(2)}) copy-start(f32[256,2]{0,1:T(2,128)} %param.22) | copy-start | bytes 6148
  211.5 34.3 %all-to-all-start.4 = ((bf16[32,20,256]{2,1,0:T(8,128)(2,1)}), bf16[32,20,256]{2,1,0:T(8,128)(2,1)S(1)}, u32[]{:S(2)}, u32[]{:S(2)}) async-start(bf16[32,20,256]{2,1,0:T(8,128)(2,1)} %reshape.137), calls=%async_computation.4 | async-start | bytes 786432 | tf_op jit(solution)/shard_map/all_to_all | solution.py:124
